TPU v7x, 32 devices: a whole 2x2x4 slice. The times are simulated.
32 devices in a mesh: sp: 8 (over z, core), tp: 4 (over y, x).
Axes of the slice: x: 2, y: 2, z: 4, core: 2. Of those that a mesh axis runs over, the one named last changes fastest.
Arguments:
- queries: bfloat16 [2048, 1024], P('sp', 'tp'), may hold values from -250 to 250
- keys_values: bfloat16 [2, 2048, 256], P(None, 'sp'), may hold values from -8 to 8
- sink_logits: float32 [16], P('tp'), may hold values from 1 to 5
- proj_weight: bfloat16 [1024, 2048], P('tp'), may hold values from -0.75 to 0.75
- residual: bfloat16 [2048, 2048], P('sp', 'tp'), may hold values from -6 to 6
- norm_gain: float32 [2048], replicated, may hold values from 0.1 to 1.9
- routes: int32 [2048, 2], P('sp'), may hold values from 0 to 7, all different within a row; in each aligned block of 256 rows (0 to 255, 256 to 511, ...) at most 128 rows name the same one
- route_weights: float32 [2048, 2], P('sp'), may hold values from 0.2 to 1
- gate_weight: bfloat16 [8, 2048, 2048], P('sp', None, 'tp'), may hold values from -0.125 to 0.125
- up_weight: bfloat16 [8, 2048, 2048], P('sp', None, 'tp'), may hold values from -0.125 to 0.125
- down_weight: bfloat16 [8, 2048, 2048], P('sp', None, 'tp'), may hold values from -0.125 to 0.125
- shared_gate: bfloat16 [2048, 2048], P(None, 'tp'), may hold values from -0.125 to 0.125
- shared_up: bfloat16 [2048, 2048], P(None, 'tp'), may hold values from -0.125 to 0.125
- shared_down: bfloat16 [2048, 2048], P(None, 'tp'), may hold values from -0.125 to 0.125
Outputs:
- output: bfloat16 [2048, 2048], P('sp', 'tp')
Inputs may be any that keep to these rules, and one draw needn't show every extreme that they name: `routes`: the 2 experts of a position differ. In each aligned block of 256 positions no expert is named by more than 128 positions, and in some block one expert is named by exactly 128.
All inputs are finite; a program needn't handle non-finite values.
Results may differ from a plain program's by a relative error of at most 0.0067.
Values may be sent and summed in bfloat16 or wider, within the bound.
A program may use at most 64 MiB of HBM per device.

v0:
```python
import jax
import jax.numpy as jnp
from jax import lax
from jax.sharding import PartitionSpec as P

D = 2048
HEADS = 16
KV_HEADS = 4
HEAD_WIDTH = 64
WINDOW = 128
TOP_K = 2
EXP_DEV = 1
TOK_DEV = 256
norm_eps = 1e-06


def passed_along(value, axis, steps):
    count = lax.axis_size(axis)
    initial, last = (max(0, -steps), min(count, count - steps))
    return lax.ppermute(value, axis, [(source, source + steps) for source in range(initial, last)])


def per_device(
    queries,
    keys_values,
    sink_logits,
    proj_weight,
    residual,
    norm_gain,
    routes,
    route_weights,
    gate_weight,
    up_weight,
    down_weight,
    shared_gate,
    shared_up,
    shared_down,
):
    tp_index = lax.axis_index("tp")
    sp_index = lax.axis_index("sp")
    sp_count = lax.axis_size("sp")
    tp_count = lax.axis_size("tp")
    heads_here = sink_logits.shape[0]
    col_width = residual.shape[1]
    blocks = TOK_DEV // WINDOW
    kv_group = HEADS // KV_HEADS
    earlier_keys = passed_along(keys_values[:, TOK_DEV - WINDOW :, :], "sp", 1)
    extended = jnp.concatenate([earlier_keys, keys_values], axis=1)
    extended = extended.reshape(2, TOK_DEV + WINDOW, KV_HEADS, HEAD_WIDTH)
    head_ids = tp_index * heads_here + jnp.arange(heads_here, dtype=jnp.int32)
    chosen = jnp.take(extended, head_ids // kv_group, axis=2)
    earlier = chosen[:, :TOK_DEV].reshape(2, blocks, WINDOW, heads_here, HEAD_WIDTH)
    later = chosen[:, WINDOW:].reshape(2, blocks, WINDOW, heads_here, HEAD_WIDTH)
    banded = jnp.concatenate([earlier, later], axis=2)
    query_blocks = queries.reshape(blocks, WINDOW, heads_here, HEAD_WIDTH)
    score_matrix = jnp.einsum(
        "bqhd,bkhd->bhqk", query_blocks, banded[0], preferred_element_type=jnp.float32
    ) * HEAD_WIDTH ** (-0.5)
    query_pos = jnp.arange(WINDOW, dtype=jnp.int32)[:, None]
    key_pos = jnp.arange(2 * WINDOW, dtype=jnp.int32)[None, :]
    distance = WINDOW + query_pos - key_pos
    absolute = (
        sp_index * TOK_DEV
        + jnp.arange(blocks, dtype=jnp.int32)[:, None, None] * WINDOW
        - WINDOW
        + key_pos[None]
    )
    allowed = (distance >= 0)[None] & (distance < WINDOW)[None] & (absolute >= 0)
    masked = jnp.where(allowed[:, None], score_matrix, -jnp.inf)
    sink_value = sink_logits[None, :, None, None]
    highest = jnp.maximum(jnp.max(masked, axis=-1, keepdims=True), sink_value)
    weights_exp = jnp.exp(masked - highest)
    denominator = jnp.sum(weights_exp, axis=-1, keepdims=True) + jnp.exp(sink_value - highest)
    softmax_weights = (weights_exp / denominator).astype(jnp.bfloat16)
    attended_values = jnp.einsum(
        "bhqk,bkhd->bqhd", softmax_weights, banded[1], preferred_element_type=jnp.float32
    )
    attended_values = attended_values.astype(jnp.bfloat16).reshape(TOK_DEV, heads_here * HEAD_WIDTH)
    attended_all = lax.all_gather(attended_values, "tp", axis=1, tiled=True)
    weight_rows = proj_weight.shape[0]
    column_share = lax.all_to_all(
        proj_weight.reshape(weight_rows, tp_count, col_width),
        "tp",
        split_axis=1,
        concat_axis=0,
        tiled=True,
    )
    column_share = column_share.reshape(HEADS * HEAD_WIDTH, col_width)
    feature_sum = jnp.dot(attended_all, column_share, preferred_element_type=jnp.float32)
    stream_cols = (feature_sum + residual.astype(jnp.float32)).astype(jnp.bfloat16)
    stream_rows = lax.all_gather(stream_cols, "tp", axis=1, tiled=True)
    gate_eff = (norm_gain[None, :, None] * gate_weight.astype(jnp.float32)).astype(jnp.bfloat16)
    up_eff = (norm_gain[None, :, None] * up_weight.astype(jnp.float32)).astype(jnp.bfloat16)
    shared_gate_eff = (norm_gain[:, None] * shared_gate.astype(jnp.float32)).astype(jnp.bfloat16)
    shared_up_eff = (norm_gain[:, None] * shared_up.astype(jnp.float32)).astype(jnp.bfloat16)
    experts_total = EXP_DEV * sp_count
    capacity = 2 * TOK_DEV * TOP_K // experts_total
    rows_per_expert = sp_count * capacity
    flat_routes = routes.reshape(-1)
    onehot = (flat_routes[:, None] == jnp.arange(experts_total, dtype=jnp.int32)[None, :]).astype(
        jnp.int32
    )
    before = jnp.cumsum(onehot, axis=0) - onehot
    slot_rank = jnp.sum(before * onehot, axis=1)
    slot_index = (
        flat_routes % EXP_DEV * rows_per_expert + flat_routes // EXP_DEV * capacity + slot_rank
    )
    token_of = jnp.arange(TOK_DEV * TOP_K, dtype=jnp.int32) // TOP_K
    slot_owner = (
        jnp.full((EXP_DEV * rows_per_expert,), TOK_DEV, jnp.int32).at[slot_index].set(token_of)
    )
    picked_rows = jnp.take(stream_rows, slot_owner, axis=0, mode="fill", fill_value=0)
    arrived = lax.all_to_all(
        picked_rows.reshape(EXP_DEV, sp_count, capacity, stream_rows.shape[1]),
        "sp",
        split_axis=1,
        concat_axis=1,
        tiled=True,
    )
    arrived = arrived.reshape(EXP_DEV, rows_per_expert, D)
    routed_squares = jnp.sum(jnp.square(arrived.astype(jnp.float32)), axis=-1)
    gate_sum = jnp.einsum("erd,edf->erf", arrived, gate_eff, preferred_element_type=jnp.float32)
    up_sum = jnp.einsum("erd,edf->erf", arrived, up_eff, preferred_element_type=jnp.float32)
    own_squares = jnp.sum(jnp.square(stream_rows.astype(jnp.float32)), axis=-1)
    shared_gate_sum = jnp.dot(stream_rows, shared_gate_eff, preferred_element_type=jnp.float32)
    shared_up_sum = jnp.dot(stream_rows, shared_up_eff, preferred_element_type=jnp.float32)
    routed_scale = lax.rsqrt(routed_squares / D + norm_eps)[..., None]
    own_scale = lax.rsqrt(own_squares / D + norm_eps)[:, None]
    hidden = (jax.nn.silu(routed_scale * gate_sum) * (routed_scale * up_sum)).astype(jnp.bfloat16)
    shared_hidden = (jax.nn.silu(own_scale * shared_gate_sum) * (own_scale * shared_up_sum)).astype(
        jnp.bfloat16
    )
    routed_piece = lax.all_gather(hidden, "tp", axis=2, tiled=True)
    own_piece = lax.all_gather(shared_hidden[None], "tp", axis=2, tiled=True)
    expert_out = jnp.einsum(
        "erf,efd->erd", routed_piece, down_weight, preferred_element_type=jnp.float32
    )
    shared_out = jnp.dot(own_piece[0], shared_down, preferred_element_type=jnp.float32)
    outgoing = expert_out.astype(jnp.bfloat16).reshape(EXP_DEV, sp_count, capacity, col_width)
    returned = lax.all_to_all(outgoing, "sp", split_axis=1, concat_axis=1, tiled=True).reshape(
        EXP_DEV * rows_per_expert, col_width
    )
    picked = jnp.take(returned, slot_index, axis=0).reshape(TOK_DEV, TOP_K, col_width)
    routed_sum = jnp.einsum("nk,nkd->nd", route_weights, picked.astype(jnp.float32))
    return (stream_cols.astype(jnp.float32) + shared_out + routed_sum).astype(jnp.bfloat16)


def solution(mesh):
    placed = (
        P("sp", "tp"),
        P(None, "sp", None),
        P("tp"),
        P("tp", None),
        P("sp", "tp"),
        P(),
        P("sp", None),
        P("sp", None),
        P("sp", None, "tp"),
        P("sp", None, "tp"),
        P("sp", None, "tp"),
        P(None, "tp"),
        P(None, "tp"),
        P(None, "tp"),
    )
    return jax.shard_map(
        per_device, mesh=mesh, in_specs=placed, out_specs=P("sp", "tp"), check_vma=False
    )
```

profile of v0, /device:TPU:0, one launch (start us, length us, event | category | flops | bytes accessed | tf_op | source)
XLA Modules:
  0.0 293.3 jit_solution(9455327325811044780)
XLA Ops:
  6.5 1.2 copy.63
  7.8 3.2 %collective-permute-start = (bf16[2,128,256]{1,2,0:T(8,128)(2,1)S(1)}, bf16[2,128,256]{1,2,0:T(8,128)(2,1)}, u32[]{:S(2)}, u32[]{:S(2)}) collective-permute-start(bf16[2,128,256]{1,2,0:T(8,128)(2,1)S(1)} %slice.34), channel_id=1, source_target_pairs={{0,4},{4,8},{8,12},{12,16},{16,20},{20,24},{24,28},{1,5},{5,9},{9,... | collective-permute-start | bytes 393224 | tf_op jit(solution)/shard_map/ppermute | solution.py:20
  11.0 2.3 copy.73
  13.3 4.5 %all-to-all-start = ((bf16[256,4,512]{0,2,1:T(8,128)(2,1)}), bf16[256,4,512]{0,2,1:T(8,128)(2,1)S(1)}, u32[]{:S(2)}, u32[]{:S(2)}) async-start(bf16[256,4,512]{0,2,1:T(8,128)(2,1)} %bitcast.91), calls=%async_computation | async-start | bytes 2097152 | tf_op jit(solution)/shard_map/all_to_all | solution.py:81
  17.8 0.1 add_compare_fusion
  18.0 0.8 broadcast_and_fusion
  18.7 0.9 reshape.384
  19.6 1.0 pad_maximum_fusion
  20.7 1.4 gather_fusion
  22.0 1.1 select_bitcast_fusion
  23.2 0.8 fusion.47
  24.0 1.0 reshape.382
  25.1 0.8 copy_dynamic-update-slice_fusion.1
  25.8 1.0 reshape.383
  26.9 0.8 copy_dynamic-update-slice_fusion
  27.6 1.5 fusion.48
  29.1 0.1 broadcast_maximum_fusion
  29.2 0.2 fusion.29
  29.4 0.1 exponential_add_fusion
  29.4 0.3 fusion.28
  29.8 0.0 copy-start.13
  29.8 0.1 copy.72
  30.0 12.7 %all_gather.12 = bf16[256,1024]{0,1:T(8,128)(2,1)} all-gather(bf16[256,256]{0,1:T(8,128)(2,1)S(1)} %bitcast.95), channel_id=1, replica_groups=mesh['sp'=8,'tp'=4] {'tp'}, dimensions={1}, use_global_device_ids=true | all-gather | bytes 655360 | tf_op jit(solution)/shard_map/all_gather | solution.py:79
  42.7 1.3 copy.74
  44.0 2.6 fusion.25
  46.6 0.0 all-gather.6.cloned.1.call-update
  46.6 0.0 all-gather.10.cloned.1.call-start
  46.7 0.1 copy.75
  46.8 0.1 eq.28
  47.0 0.1 reshape.334
  47.1 1.1 reduce-window.6
  48.3 0.2 slice_reduce_fusion
  48.5 0.1 copy.79
  48.7 0.2 mul.142
  48.8 0.1 fusion.37
  48.9 2.4 scatter_custom_fusion
  51.4 20.4 %all-gather.6.cloned.1.call-done = bf16[256,2048]{1,0:T(8,128)(2,1)} async-done(((bf16[256,512]{1,0:T(8,128)(2,1)}), bf16[256,2048]{1,0:T(8,128)(2,1)}) %all-gather.6.cloned.1.call-update) | async-done | bytes 1048592 | tf_op jit(solution)/shard_map/all_gather | solution.py:91
  71.8 10.2 %gather_fusion.1 = bf16[1024,2048]{1,0:T(8,128)(2,1)} fusion(bf16[256,2048]{1,0:T(8,128)(2,1)} %all-gather.6.cloned.1.call-done, s32[1024]{0:T(1024)S(1)} %fusion.39), kind=kCustom, calls=%fused_computation.1 | custom fusion | bytes 8392704 | tf_op jit(solution)/shard_map/jit(_take)/gather | solution.py:112
  82.0 2.5 broadcast_select_fusion
  84.5 98.4 %all_to_all.25 = bf16[1,8,128,2048]{3,2,0,1:T(8,128)(2,1)S(1)} all-to-all(bf16[1,8,128,2048]{3,2,0,1:T(8,128)(2,1)S(1)} %broadcast_select_fusion), channel_id=1, replica_groups=mesh['sp'=8,'tp'=4] {'sp'}, dimensions={1} | all-to-all | bytes 8388608 | tf_op jit(solution)/shard_map/all_to_all | solution.py:113
  182.9 0.9 multiply_reduce_fusion
  183.8 0.7 copy-done.10
  184.5 2.4 fusion.3
  186.9 3.7 %multiply_convert_fusion.6 = bf16[1024,512]{1,0:T(8,128)(2,1)} fusion(f32[1024,512]{1,0:T(8,128)S(1)} %fusion.3, bf16[1024,2048]{1,0:T(8,128)(2,1)S(1)} %bitcast.89, bf16[1,2048,512]{2,1,0:T(8,128)(2,1)S(1)} %copy-done.11, f32[2048]{0:T(1024)S(1)} %copy-done.14, f32[1024]{0:T(1024)S(1)} %rsqrt_bitcast_fusion), kind=kOutput, calls=%fused_computation.18 | convolution fusion | flops 2154823680 | bytes 9449472 | tf_op jit(solution)/shard_map/erd,edf->erf/dot_general | solution.py:123
  190.7 0.0 all-gather.10.cloned.1.call-update
  190.7 0.3 multiply_reduce_fusion.1
  191.0 50.3 %all-gather.10.cloned.1.call-done = bf16[1024,2048]{1,0:T(8,128)(2,1)} async-done(((bf16[1024,512]{1,0:T(8,128)(2,1)}), bf16[1024,2048]{1,0:T(8,128)(2,1)}) %all-gather.10.cloned.1.call-update) | async-done | bytes 4194320 | tf_op jit(solution)/shard_map/all_gather | solution.py:133
  241.3 5.5 %fusion.16 = bf16[1024,512]{1,0:T(8,128)(2,1)} fusion(bf16[1024,2048]{1,0:T(8,128)(2,1)} %all-gather.10.cloned.1.call-done, bf16[1,2048,512]{2,1,0:T(8,128)(2,1)S(1)} %copy-done), kind=kOutput, calls=%fused_computation.24 | convolution fusion | flops 2148007936 | bytes 7340032 | tf_op jit(solution)/shard_map/erf,efd->erd/dot_general | solution.py:135
  246.8 4.6 %all-to-all-start.2 = ((bf16[1,8,128,512]{3,2,0,1:T(8,128)(2,1)}), bf16[1,8,128,512]{3,2,0,1:T(8,128)(2,1)}, u32[]{:S(2)}, u32[]{:S(2)}) async-start(bf16[1,8,128,512]{3,2,0,1:T(8,128)(2,1)} %bitcast.93), calls=%async_computation.2 | async-start | bytes 2097152 | tf_op jit(solution)/shard_map/all_to_all | solution.py:140
  251.4 0.0 all-gather.8.cloned.1.call-start
  251.4 0.0 copy-start.12
  251.4 2.6 fusion.23
  254.0 0.0 copy-start.8
  254.0 1.6 fusion.27
  255.6 0.0 all-gather.8.cloned.1.call-update
  255.6 0.1 reduce_sum.43
  255.8 0.1 copy.77
  255.9 0.2 copy.78
  256.1 0.2 copy.83
  256.3 21.8 %all-to-all-done.2 = bf16[1,8,128,512]{3,2,0,1:T(8,128)(2,1)} async-done(((bf16[1,8,128,512]{3,2,0,1:T(8,128)(2,1)}), bf16[1,8,128,512]{3,2,0,1:T(8,128)(2,1)}, u32[]{:S(2)}, u32[]{:S(2)}) %all-to-all-start.2) | async-done | bytes 1048608 | tf_op jit(solution)/shard_map/all_to_all | solution.py:140
  278.0 3.3 %gather_fusion.2 = bf16[512,512]{1,0:T(8,128)(2,1)S(1)} fusion(bf16[1024,512]{1,0:T(8,128)(2,1)} %bitcast.25, s32[1024]{0:T(1024)S(1)} %pad_clamp_fusion), kind=kCustom, calls=%fused_computation.2 | custom fusion | bytes 1050624 | tf_op jit(solution)/shard_map/jit(_take)/gather | solution.py:143
  281.4 0.2 gather.20
  281.6 1.8 fusion.30
  283.4 3.4 %fusion.26 = bf16[256,512]{1,0:T(8,128)(2,1)} fusion(bf16[256,2048]{1,0:T(8,128)(2,1)} %all-gather.8.cloned.1.call-done, bf16[2048,512]{1,0:T(8,128)(2,1)} %param.27, f32[256,1,512]{2,1,0:T(1,128)} %fusion.30, bf16[256,512]{1,0:T(8,128)(2,1)S(1)} %copy-done.3), kind=kOutput, calls=%fused_computation.35 | convolution fusion | flops 537395200 | bytes 4194304 | tf_op jit(solution)/shard_map/dot_general | solution.py:138
  (50 shorter events, 0.3 us)
Async XLA Ops:
  6.5 234.7 %copy-start = (bf16[1,2048,512]{2,1,0:T(8,128)(2,1)S(1)}, bf16[1,2048,512]{2,1,0:T(8,128)(2,1)}, u32[]{:S(2)}) copy-start(bf16[1,2048,512]{2,1,0:T(8,128)(2,1)} %param.24) | copy-start | bytes 6291460
  7.8 5.5 %copy-start.2 = (bf16[2,256,256]{1,2,0:T(8,128)(2,1)}, bf16[2,256,256]{1,2,0:T(8,128)(2,1)S(1)}, u32[]{:S(2)}) copy-start(bf16[2,256,256]{1,2,0:T(8,128)(2,1)S(1)} %copy.63) | copy-start | bytes 786436
  7.8 10.9 %copy-start.4 = (bf16[256,256]{1,0:T(8,128)(2,1)S(1)}, bf16[256,256]{1,0:T(8,128)(2,1)}, u32[]{:S(2)}) copy-start(bf16[256,256]{1,0:T(8,128)(2,1)} %param.14) | copy-start | bytes 393220
  7.8 11.8 %collective-permute-start = (bf16[2,128,256]{1,2,0:T(8,128)(2,1)S(1)}, bf16[2,128,256]{1,2,0:T(8,128)(2,1)}, u32[]{:S(2)}, u32[]{:S(2)}) collective-permute-start(bf16[2,128,256]{1,2,0:T(8,128)(2,1)S(1)} %slice.34), channel_id=1, source_target_pairs={{0,4},{4,8},{8,12},{12,16},{16,20},{20,24},{24,28},{1,5},{5,9},{9,... | collective-permute-start | bytes 393224 | tf_op jit(solution)/shard_map/ppermute | solution.py:20
  13.3 29.4 %all-to-all-start = ((bf16[256,4,512]{0,2,1:T(8,128)(2,1)}), bf16[256,4,512]{0,2,1:T(8,128)(2,1)S(1)}, u32[]{:S(2)}, u32[]{:S(2)}) async-start(bf16[256,4,512]{0,2,1:T(8,128)(2,1)} %bitcast.91), calls=%async_computation | async-start | bytes 2097152 | tf_op jit(solution)/shard_map/all_to_all | solution.py:81
  17.8 54.0 %all-gather.6.cloned.1.call-start = ((), (), s32[]{:S(2)}) async-start(), calls=%async_computation.3 | async-start | bytes 1310720 | tf_op jit(solution)/shard_map/all_gather | solution.py:91
  22.0 5.6 %copy-start.6 = (pred[2,128,256]{1,2,0:T(8,128)(4,1)S(1)}, pred[2,128,256]{1,2,0:T(8,128)(4,1)}, u32[]{:S(2)}) copy-start(pred[2,128,256]{1,2,0:T(8,128)(4,1)} %broadcast_and_fusion) | copy-start | bytes 196612
  24.0 5.1 %copy-start.9 = (f32[4]{0:T(128)S(1)}, f32[4]{0:T(128)}, u32[]{:S(2)}) copy-start(f32[4]{0:T(128)} %param.16) | copy-start | bytes 52
  27.6 1.8 copy-start.5
  29.8 14.3 %copy-start.13 = (bf16[256,512]{1,0:T(8,128)(2,1)S(1)}, bf16[256,512]{1,0:T(8,128)(2,1)}, u32[]{:S(2)}) copy-start(bf16[256,512]{1,0:T(8,128)(2,1)} %param.18) | copy-start | bytes 786436
  42.7 4.0 %copy-start.7 = (s32[256,2]{0,1:T(2,128)S(1)}, s32[256,2]{0,1:T(2,128)}, u32[]{:S(2)}) copy-start(s32[256,2]{0,1:T(2,128)} %param.20) | copy-start | bytes 6148
  46.6 194.7 %all-gather.10.cloned.1.call-start = ((), (), s32[]{:S(2)}) async-start(), calls=%async_computation.5 | async-start | bytes 5242880 | tf_op jit(solution)/shard_map/all_gather | solution.py:133
  182.9 1.6 copy-start.10
  182.9 1.6 copy-start.14
  184.5 2.4 copy-start.11
  186.9 3.8 %copy-start.1 = (bf16[256,2048]{1,0:T(8,128)(2,1)S(1)}, bf16[256,2048]{1,0:T(8,128)(2,1)}, u32[]{:S(2)}) copy-start(bf16[256,2048]{1,0:T(8,128)(2,1)} %all-gather.6.cloned.1.call-done) | copy-start | bytes 3145732
  246.8 31.3 %all-to-all-start.2 = ((bf16[1,8,128,512]{3,2,0,1:T(8,128)(2,1)}), bf16[1,8,128,512]{3,2,0,1:T(8,128)(2,1)}, u32[]{:S(2)}, u32[]{:S(2)}) async-start(bf16[1,8,128,512]{3,2,0,1:T(8,128)(2,1)} %bitcast.93), calls=%async_computation.2 | async-start | bytes 2097152 | tf_op jit(solution)/shard_map/all_to_all | solution.py:140
  251.4 32.0 %all-gather.8.cloned.1.call-start = ((), (), s32[]{:S(2)}) async-start(), calls=%async_computation.4 | async-start | bytes 1310720 | tf_op jit(solution)/shard_map/all_gather | solution.py:134
  251.4 2.6 copy-start.12
  254.0 2.1 copy-start.8
  281.6 1.8 copy-start.3
Sparse Core Ops, SparseCore 0:
  46.7 25.0 all-gather.5
  190.8 50.3 all-gather.9
  255.8 26.7 all-gather.7
where the time goes:
time: 294 us; the launch traced here: 293 us
  blocking collectives  111 us (38%)
  waiting for transfers between devices  92.4 us (31%)
  local copies, waits for them, and re-layouts  30.1 us (10%)
  matrix products  25.3 us (9%)
  between operations  13.5 us (5%)
  starting transfers between devices  12.4 us (4%)
  other arithmetic  8.46 us (3%)
    all_to_all x1, blocking collectives, per_device(): lax.all_to_all(picked_rows.reshape(EXP_DEV, sp_count, capacity, stream_ro...  98.4 us
    all_gather x1, waiting for transfers between devices, per_device(): routed_piece = lax.all_gather(hidden, 'tp', axis=2, tiled=True)  50.3 us
    all_to_all x1, waiting for transfers between devices, per_device(): lax.all_to_all(outgoing, 'sp', split_axis=1, concat_axis=1, tiled=True)  21.8 us
    all_gather x1, waiting for transfers between devices, per_device(): stream_rows = lax.all_gather(stream_cols, 'tp', axis=1, tiled=True)  20.4 us
    all_gather x1, blocking collectives, per_device(): attended_all = lax.all_gather(attended_values, 'tp', axis=1, tiled=True)  12.7 us
    gather x1, local copies, waits for them, and re-layouts, per_device(): jnp.take(stream_rows, slot_owner, axis=0, mode='fill', fill_value=0)  10.2 us
  transfers between devices with their start and end apart: 6, of which 3 were waited for; matrix products, arithmetic and copies ran while one was open for 10% of the time, Pallas kernels for 0%

commit v1 on v0

--- a/solution.py
+++ b/solution.py
@@ -110,12 +110,20 @@
         jnp.full((EXP_DEV * rows_per_expert,), TOK_DEV, jnp.int32).at[slot_index].set(token_of)
     )
     picked_rows = jnp.take(stream_rows, slot_owner, axis=0, mode="fill", fill_value=0)
-    arrived = lax.all_to_all(
-        picked_rows.reshape(EXP_DEV, sp_count, capacity, stream_rows.shape[1]),
-        "sp",
-        split_axis=1,
-        concat_axis=1,
-        tiled=True,
+    arrived = jnp.concatenate(
+        lax.all_to_all(
+            jnp.stack(
+                jnp.split(
+                    picked_rows.reshape(EXP_DEV, sp_count, capacity, stream_rows.shape[1]),
+                    lax.axis_size("sp"),
+                    axis=1,
+                )
+            ),
+            "sp",
+            0,
+            0,
+        ),
+        axis=1,
     )
     arrived = arrived.reshape(EXP_DEV, rows_per_expert, D)
     routed_squares = jnp.sum(jnp.square(arrived.astype(jnp.float32)), axis=-1)

time: 294 us -> 295 us (level)
  no operation moved by 1% of the time
where the time goes in v1:
time: 295 us; the launch traced here: 294 us
  blocking collectives  111 us (38%)
  waiting for transfers between devices  91.9 us (31%)
  local copies, waits for them, and re-layouts  31 us (11%)
  matrix products  26.2 us (9%)
  between operations  13.5 us (5%)
  starting transfers between devices  12.3 us (4%)
  other arithmetic  8.42 us (3%)
    all_to_all x1, blocking collectives, per_device(): lax.all_to_all(jnp.stack(jnp.split(picked_rows.reshape(EXP_DEV, sp_count,...  98.4 us
    all_gather x1, waiting for transfers between devices, per_device(): routed_piece = lax.all_gather(hidden, 'tp', axis=2, tiled=True)  50.3 us
    all_to_all x1, waiting for transfers between devices, per_device(): lax.all_to_all(outgoing, 'sp', split_axis=1, concat_axis=1, tiled=True)  21.2 us
    all_gather x1, waiting for transfers between devices, per_device(): stream_rows = lax.all_gather(stream_cols, 'tp', axis=1, tiled=True)  20.4 us
    all_gather x1, blocking collectives, per_device(): attended_all = lax.all_gather(attended_values, 'tp', axis=1, tiled=True)  12.8 us
    gather x1, local copies, waits for them, and re-layouts, per_device(): jnp.take(stream_rows, slot_owner, axis=0, mode='fill', fill_value=0)  10.2 us
  transfers between devices with their start and end apart: 6, of which 3 were waited for; matrix products, arithmetic and copies ran while one was open for 10% of the time, Pallas kernels for 0%

profile of v1, /device:TPU:0, one launch (start us, length us, event | category | flops | bytes accessed | tf_op | source)
XLA Modules:
  0.0 294.4 jit_solution(4029410759388592115)
XLA Ops:
  6.5 1.2 copy.62
  7.8 3.1 %collective-permute-start = (bf16[2,128,256]{1,2,0:T(8,128)(2,1)S(1)}, bf16[2,128,256]{1,2,0:T(8,128)(2,1)}, u32[]{:S(2)}, u32[]{:S(2)}) collective-permute-start(bf16[2,128,256]{1,2,0:T(8,128)(2,1)S(1)} %slice.34), channel_id=1, source_target_pairs={{0,4},{4,8},{8,12},{12,16},{16,20},{20,24},{24,28},{1,5},{5,9},{9,... | collective-permute-start | bytes 393224 | tf_op jit(solution)/shard_map/ppermute | solution.py:20
  10.9 2.2 copy.72
  13.1 4.5 %all-to-all-start = ((bf16[256,4,512]{0,2,1:T(8,128)(2,1)}), bf16[256,4,512]{0,2,1:T(8,128)(2,1)S(1)}, u32[]{:S(2)}, u32[]{:S(2)}) async-start(bf16[256,4,512]{0,2,1:T(8,128)(2,1)} %bitcast.121), calls=%async_computation | async-start | bytes 2097152 | tf_op jit(solution)/shard_map/all_to_all | solution.py:81
  17.7 0.1 add_compare_fusion
  17.8 0.8 broadcast_and_fusion
  18.6 0.0 copy-start.7
  18.6 0.9 reshape.383
  19.5 1.0 pad_maximum_fusion
  20.5 1.4 gather_fusion
  21.9 1.1 select_bitcast_fusion
  23.0 0.9 fusion.55
  23.9 1.0 reshape.381
  24.9 0.8 copy_dynamic-update-slice_fusion.1
  25.7 1.0 reshape.382
  26.7 0.8 copy_dynamic-update-slice_fusion
  27.5 1.4 fusion.56
  28.9 0.1 broadcast_maximum_fusion
  29.0 0.2 fusion.29
  29.1 0.1 exponential_add_fusion
  29.2 1.3 fusion.28
  30.5 0.1 copy.71
  30.7 12.8 %all_gather.12 = bf16[256,1024]{0,1:T(8,128)(2,1)} all-gather(bf16[256,256]{0,1:T(8,128)(2,1)S(1)} %bitcast.125), channel_id=1, replica_groups=mesh['sp'=8,'tp'=4] {'tp'}, dimensions={1}, use_global_device_ids=true | all-gather | bytes 655360 | tf_op jit(solution)/shard_map/all_gather | solution.py:79
  43.4 1.3 copy.73
  44.8 2.6 fusion.25
  47.3 0.0 all-gather.6.cloned.1.call-update
  47.3 0.0 all-gather.10.cloned.1.call-start
  47.4 0.1 copy.74
  47.5 0.1 eq.28
  47.7 0.1 reshape.333
  47.8 1.1 reduce-window.6
  49.0 0.2 slice_reduce_fusion
  49.2 0.1 copy.78
  49.4 0.2 mul.142
  49.5 0.1 fusion.45
  49.6 2.4 scatter_custom_fusion
  52.1 20.4 %all-gather.6.cloned.1.call-done = bf16[256,2048]{1,0:T(8,128)(2,1)} async-done(((bf16[256,512]{1,0:T(8,128)(2,1)}), bf16[256,2048]{1,0:T(8,128)(2,1)}) %all-gather.6.cloned.1.call-update) | async-done | bytes 1048592 | tf_op jit(solution)/shard_map/all_gather | solution.py:91
  72.5 10.2 %gather_fusion.1 = bf16[1024,2048]{1,0:T(8,128)(2,1)} fusion(bf16[256,2048]{1,0:T(8,128)(2,1)} %all-gather.6.cloned.1.call-done, s32[1024]{0:T(1024)S(1)} %fusion.47), kind=kCustom, calls=%fused_computation.1 | custom fusion | bytes 8392704 | tf_op jit(solution)/shard_map/jit(_take)/gather | solution.py:112
  82.6 2.5 broadcast_select_fusion
  85.5 98.4 %all_to_all.25 = bf16[8,1,1,128,2048]{4,3,2,1,0:T(8,128)(2,1)S(1)} all-to-all(bf16[8,1,1,128,2048]{4,3,2,1,0:T(8,128)(2,1)S(1)} %fusion.30), channel_id=1, replica_groups=mesh['sp'=8,'tp'=4] {'sp'}, dimensions={0} | all-to-all | bytes 8388608 | tf_op jit(solution)/shard_map/all_to_all | solution.py:114
  183.9 0.9 multiply_reduce_fusion
  184.8 0.7 copy-done.8
  185.5 2.4 fusion.3
  188.0 3.7 %multiply_convert_fusion.6 = bf16[1024,512]{1,0:T(8,128)(2,1)} fusion(f32[1024,512]{1,0:T(8,128)S(1)} %fusion.3, bf16[1024,2048]{1,0:T(8,128)(2,1)S(1)} %bitcast.119, bf16[1,2048,512]{2,1,0:T(8,128)(2,1)S(1)} %copy-done.9, f32[2048]{0:T(1024)S(1)} %copy-done.12, f32[1024]{0:T(1024)S(1)} %rsqrt_bitcast_fusion), kind=kOutput, calls=%fused_computation.18 | convolution fusion | flops 2154823680 | bytes 9449472 | tf_op jit(solution)/shard_map/erd,edf->erf/dot_general | solution.py:131
  191.7 0.0 all-gather.10.cloned.1.call-update
  191.8 0.3 multiply_reduce_fusion.1
  192.1 50.3 %all-gather.10.cloned.1.call-done = bf16[1024,2048]{1,0:T(8,128)(2,1)} async-done(((bf16[1024,512]{1,0:T(8,128)(2,1)}), bf16[1024,2048]{1,0:T(8,128)(2,1)}) %all-gather.10.cloned.1.call-update) | async-done | bytes 4194320 | tf_op jit(solution)/shard_map/all_gather | solution.py:141
  242.3 5.5 %fusion.16 = bf16[1024,512]{1,0:T(8,128)(2,1)} fusion(bf16[1024,2048]{1,0:T(8,128)(2,1)} %all-gather.10.cloned.1.call-done, bf16[1,2048,512]{2,1,0:T(8,128)(2,1)S(1)} %copy-done), kind=kOutput, calls=%fused_computation.24 | convolution fusion | flops 2148007936 | bytes 7340032 | tf_op jit(solution)/shard_map/erf,efd->erd/dot_general | solution.py:143
  247.8 4.6 %all-to-all-start.2 = ((bf16[1,8,128,512]{3,2,0,1:T(8,128)(2,1)}), bf16[1,8,128,512]{3,2,0,1:T(8,128)(2,1)}, u32[]{:S(2)}, u32[]{:S(2)}) async-start(bf16[1,8,128,512]{3,2,0,1:T(8,128)(2,1)} %bitcast.123), calls=%async_computation.2 | async-start | bytes 2097152 | tf_op jit(solution)/shard_map/all_to_all | solution.py:148
  252.4 0.0 all-gather.8.cloned.1.call-start
  252.4 0.0 copy-start.10
  252.5 2.6 fusion.23
  255.1 1.6 fusion.27
  256.7 0.0 all-gather.8.cloned.1.call-update
  256.7 0.1 reduce_sum.43
  256.8 0.1 copy.76
  256.9 0.8 copy.77
  257.7 0.2 copy.81
  257.9 21.2 %all-to-all-done.2 = bf16[1,8,128,512]{3,2,0,1:T(8,128)(2,1)} async-done(((bf16[1,8,128,512]{3,2,0,1:T(8,128)(2,1)}), bf16[1,8,128,512]{3,2,0,1:T(8,128)(2,1)}, u32[]{:S(2)}, u32[]{:S(2)}) %all-to-all-start.2) | async-done | bytes 1048608 | tf_op jit(solution)/shard_map/all_to_all | solution.py:148
  279.1 3.4 %gather_fusion.2 = bf16[512,512]{1,0:T(8,128)(2,1)S(1)} fusion(bf16[1024,512]{1,0:T(8,128)(2,1)} %bitcast.32, s32[1024]{0:T(1024)S(1)} %pad_clamp_fusion), kind=kCustom, calls=%fused_computation.2 | custom fusion | bytes 1050624 | tf_op jit(solution)/shard_map/jit(_take)/gather | solution.py:151
  282.5 0.2 gather.20
  282.7 1.8 fusion.38
  284.5 0.0 all-gather.8.cloned.1.call-done
  284.5 3.3 %fusion.26 = bf16[256,512]{1,0:T(8,128)(2,1)} fusion(bf16[256,2048]{1,0:T(8,128)(2,1)} %all-gather.8.cloned.1.call-done, bf16[2048,512]{1,0:T(8,128)(2,1)} %param.27, f32[256,1,512]{2,1,0:T(1,128)S(1)} %fusion.38, bf16[256,512]{1,0:T(8,128)(2,1)S(1)} %copy-done.3), kind=kOutput, calls=%fused_computation.35 | convolution fusion | flops 537395200 | bytes 4194304 | tf_op jit(solution)/shard_map/dot_general | solution.py:146
  (54 shorter events, 0.6 us)
Async XLA Ops:
  6.5 235.8 %copy-start = (bf16[1,2048,512]{2,1,0:T(8,128)(2,1)S(1)}, bf16[1,2048,512]{2,1,0:T(8,128)(2,1)}, u32[]{:S(2)}) copy-start(bf16[1,2048,512]{2,1,0:T(8,128)(2,1)} %param.24) | copy-start | bytes 6291460
  6.5 12.1 %copy-start.4 = (bf16[256,256]{1,0:T(8,128)(2,1)S(1)}, bf16[256,256]{1,0:T(8,128)(2,1)}, u32[]{:S(2)}) copy-start(bf16[256,256]{1,0:T(8,128)(2,1)} %param.14) | copy-start | bytes 393220
  7.8 5.3 %copy-start.2 = (bf16[2,256,256]{1,2,0:T(8,128)(2,1)}, bf16[2,256,256]{1,2,0:T(8,128)(2,1)S(1)}, u32[]{:S(2)}) copy-start(bf16[2,256,256]{1,2,0:T(8,128)(2,1)S(1)} %copy.62) | copy-start | bytes 786436
  7.8 11.7 %collective-permute-start = (bf16[2,128,256]{1,2,0:T(8,128)(2,1)S(1)}, bf16[2,128,256]{1,2,0:T(8,128)(2,1)}, u32[]{:S(2)}, u32[]{:S(2)}) collective-permute-start(bf16[2,128,256]{1,2,0:T(8,128)(2,1)S(1)} %slice.34), channel_id=1, source_target_pairs={{0,4},{4,8},{8,12},{12,16},{16,20},{20,24},{24,28},{1,5},{5,9},{9,... | collective-permute-start | bytes 393224 | tf_op jit(solution)/shard_map/ppermute | solution.py:20
  13.1 30.3 %all-to-all-start = ((bf16[256,4,512]{0,2,1:T(8,128)(2,1)}), bf16[256,4,512]{0,2,1:T(8,128)(2,1)S(1)}, u32[]{:S(2)}, u32[]{:S(2)}) async-start(bf16[256,4,512]{0,2,1:T(8,128)(2,1)} %bitcast.121), calls=%async_computation | async-start | bytes 2097152 | tf_op jit(solution)/shard_map/all_to_all | solution.py:81
  17.7 54.8 %all-gather.6.cloned.1.call-start = ((), (), s32[]{:S(2)}) async-start(), calls=%async_computation.3 | async-start | bytes 1310720 | tf_op jit(solution)/shard_map/all_gather | solution.py:91
  18.6 10.3 %copy-start.7 = (f32[4]{0:T(128)S(1)}, f32[4]{0:T(128)}, u32[]{:S(2)}) copy-start(f32[4]{0:T(128)} %param.16) | copy-start | bytes 52
  29.0 15.8 %copy-start.11 = (bf16[256,512]{1,0:T(8,128)(2,1)S(1)}, bf16[256,512]{1,0:T(8,128)(2,1)}, u32[]{:S(2)}) copy-start(bf16[256,512]{1,0:T(8,128)(2,1)} %param.18) | copy-start | bytes 786436
  29.2 18.2 %copy-start.5 = (s32[256,2]{0,1:T(2,128)S(1)}, s32[256,2]{0,1:T(2,128)}, u32[]{:S(2)}) copy-start(s32[256,2]{0,1:T(2,128)} %param.20) | copy-start | bytes 6148
  47.3 195.0 %all-gather.10.cloned.1.call-start = ((), (), s32[]{:S(2)}) async-start(), calls=%async_computation.5 | async-start | bytes 5242880 | tf_op jit(solution)/shard_map/all_gather | solution.py:141
  183.9 1.6 copy-start.8
  183.9 1.6 copy-start.12
  185.5 2.4 copy-start.9
  188.0 3.8 %copy-start.1 = (bf16[256,2048]{1,0:T(8,128)(2,1)S(1)}, bf16[256,2048]{1,0:T(8,128)(2,1)}, u32[]{:S(2)}) copy-start(bf16[256,2048]{1,0:T(8,128)(2,1)} %all-gather.6.cloned.1.call-done) | copy-start | bytes 3145732
  247.8 31.3 %all-to-all-start.2 = ((bf16[1,8,128,512]{3,2,0,1:T(8,128)(2,1)}), bf16[1,8,128,512]{3,2,0,1:T(8,128)(2,1)}, u32[]{:S(2)}, u32[]{:S(2)}) async-start(bf16[1,8,128,512]{3,2,0,1:T(8,128)(2,1)} %bitcast.123), calls=%async_computation.2 | async-start | bytes 2097152 | tf_op jit(solution)/shard_map/all_to_all | solution.py:148
  252.4 32.1 %all-gather.8.cloned.1.call-start = ((), (), s32[]{:S(2)}) async-start(), calls=%async_computation.4 | async-start | bytes 1310720 | tf_op jit(solution)/shard_map/all_gather | solution.py:142
  252.4 2.6 copy-start.10
  255.0 2.7 copy-start.6
  279.1 5.4 %copy-start.3 = (bf16[256,512]{1,0:T(8,128)(2,1)S(1)}, bf16[256,512]{1,0:T(8,128)(2,1)}, u32[]{:S(2)}) copy-start(bf16[256,512]{1,0:T(8,128)(2,1)} %fusion.25) | copy-start | bytes 786436
Sparse Core Ops, SparseCore 0:
  47.4 24.9 all-gather.5
  191.9 50.3 all-gather.9
  256.8 26.7 all-gather.7
